TPU v7x, 32 devices: a whole 2x2x4 slice. The times are simulated.
32 devices in a mesh: sp: 8 (over z, x), tp: 4 (over y, core).
Axes of the slice: x: 2, y: 2, z: 4, core: 2. Of those that a mesh axis runs over, the one named last changes fastest.
Arguments:
- tokens: bfloat16 [4096, 2048], P('sp', 'tp'), may hold values from -6 to 6
- norm_gain: float32 [2048], replicated, may hold values from 0.1 to 1.9
- w_query: bfloat16 [2048, 1024], P('sp', 'tp'), may hold values from -1 to 1
- w_key: bfloat16 [2048, 256], P('sp', 'tp'), may hold values from -16 to 16
- w_value: bfloat16 [2048, 256], P('sp', 'tp'), may hold values from -1 to 1
- w_post_gate: bfloat16 [2048, 1024], P('sp', 'tp'), may hold values from -0.125 to 0.125
- w_pre_gate: bfloat16 [2048, 1024], P('sp', 'tp'), may hold values from -0.125 to 0.125
- w_conv_in: bfloat16 [2048, 1024], P('sp', 'tp'), may hold values from -0.125 to 0.125
- conv_taps: float32 [3, 1024], P(None, 'tp'), may hold values from -3 to 3
- sink_logit: float32 [16], P('tp'), may hold values from 2 to 6
- w_out_attn: bfloat16 [1024, 2048], P('tp', 'sp'), may hold values from -0.1875 to 0.1875
- w_out_conv: bfloat16 [1024, 2048], P('tp', 'sp'), may hold values from -0.1875 to 0.1875
Outputs:
- mixed: bfloat16 [4096, 2048], P(('sp', 'tp'))
- log_weight_sum: float32 [16, 4096], P('tp', 'sp')
All inputs are finite; a program needn't handle non-finite values.
Results may differ from a plain program's by a relative error of at most 0.012.
The roundings to bfloat16 on the way count: a program that leaves them out, or rounds other values in their place, can miss the bound.
Values may be sent and summed in bfloat16 or wider, within the bound.
A program may use at most 64 MiB of HBM per device.

v0:
```python
import jax
import jax.numpy as jnp
from jax import lax
from jax.sharding import PartitionSpec as P

HEAD_DIM = 64
WINDOW = 128
GRID_W = 64
rope_base = 10000.0
norm_eps = 1e-06


def padded(block, sides, width):
    for axis, dim in sides:
        count = lax.axis_size(axis)
        forward = [(i, i + 1) for i in range(count - 1)]
        backward = [(target, source) for source, target in forward]
        low = lax.ppermute(
            lax.slice_in_dim(block, block.shape[dim] - width, None, axis=dim), axis, forward
        )
        high = lax.ppermute(lax.slice_in_dim(block, 0, width, axis=dim), axis, backward)
        block = jnp.concatenate([low, block, high], axis=dim)
    return block


def rotate_pair(values, angles):
    first_half, second_half = jnp.split(values, 2, axis=-1)
    cosine = jnp.cos(angles)[:, None, :]
    sine_part = jnp.sin(angles)[:, None, :]
    return jnp.concatenate(
        [
            first_half * cosine - second_half * sine_part,
            first_half * sine_part + second_half * cosine,
        ],
        axis=-1,
    )


def axial_rotate(values, positions):
    half_dim = values.shape[-1] // 2
    inv_freq = rope_base ** (-jnp.arange(0, half_dim, 2).astype(jnp.float32) / half_dim)
    row_angle = (positions // GRID_W).astype(jnp.float32)[:, None] * inv_freq
    col_angle = (positions % GRID_W).astype(jnp.float32)[:, None] * inv_freq
    row_part, col_part = jnp.split(values, 2, axis=-1)
    return jnp.concatenate(
        [rotate_pair(row_part, row_angle), rotate_pair(col_part, col_angle)], axis=-1
    )


def block_windows(source, rows_local, blocks):
    pieces = [
        source[step * WINDOW : step * WINDOW + rows_local].reshape(
            (blocks, WINDOW) + source.shape[1:]
        )
        for step in range(3)
    ]
    return jnp.concatenate(pieces, axis=1)


def on_device(
    tokens,
    norm_gain,
    w_query,
    w_key,
    w_value,
    w_post_gate,
    w_pre_gate,
    w_conv_in,
    conv_taps,
    sink_logit,
    w_out_attn,
    w_out_conv,
):
    whole = lax.all_gather(tokens, "tp", axis=1, tiled=True)
    rows_local = whole.shape[0]
    whole_float = whole.astype(jnp.float32)
    mean_square = jnp.mean(whole_float * whole_float, axis=1, keepdims=True)
    normed = (whole_float * lax.rsqrt(mean_square + norm_eps) * norm_gain).astype(jnp.bfloat16)
    col_widths = [
        w_query.shape[1],
        w_key.shape[1],
        w_value.shape[1],
        w_post_gate.shape[1],
        w_pre_gate.shape[1],
        w_conv_in.shape[1],
    ]
    joined = jnp.concatenate(
        (
            lax.all_gather(w_query, "sp", axis=0, tiled=True),
            lax.all_gather(w_key, "sp", axis=0, tiled=True),
            lax.all_gather(w_value, "sp", axis=0, tiled=True),
            lax.all_gather(w_post_gate, "sp", axis=0, tiled=True),
            lax.all_gather(w_pre_gate, "sp", axis=0, tiled=True),
            lax.all_gather(w_conv_in, "sp", axis=0, tiled=True),
        ),
        axis=1,
    )
    projected = jnp.dot(normed, joined, preferred_element_type=jnp.float32)
    bounds = []
    running = 0
    for col_width in col_widths[:-1]:
        running += col_width
        bounds.append(running)
    query_raw, key_raw, value_raw, post_gate, pre_gate, conv_input = jnp.split(
        projected, bounds, axis=1
    )
    offset = lax.axis_index("sp") * rows_local
    positions = offset + jnp.arange(rows_local, dtype=jnp.int32)
    local_heads = w_query.shape[1] // HEAD_DIM
    local_groups = w_key.shape[1] // HEAD_DIM
    group_size = local_heads // local_groups
    queries = axial_rotate(query_raw.reshape(rows_local, local_heads, HEAD_DIM), positions).astype(
        jnp.bfloat16
    )
    keys_rot = axial_rotate(key_raw.reshape(rows_local, local_groups, HEAD_DIM), positions).astype(
        jnp.bfloat16
    )
    key_value = jnp.concatenate(
        [keys_rot.reshape(rows_local, local_groups * HEAD_DIM), value_raw.astype(jnp.bfloat16)],
        axis=1,
    )
    mixed_input = (pre_gate * conv_input).astype(jnp.bfloat16)
    kv_padded = padded(key_value, (("sp", 0),), WINDOW)
    conv_padded = padded(mixed_input, (("sp", 0),), 1)
    conv_float = conv_padded.astype(jnp.float32)
    convolved = (
        conv_taps[0] * conv_float[:-2]
        + conv_taps[1] * conv_float[1:-1]
        + conv_taps[2] * conv_float[2:]
    )
    conv_out = (post_gate * convolved).astype(jnp.bfloat16)
    total_tokens = rows_local * lax.axis_size("sp")
    blocks = rows_local // WINDOW
    padded_rows = rows_local + 2 * WINDOW
    block_queries = queries.reshape(blocks, WINDOW, local_groups, group_size, HEAD_DIM)
    block_keys = block_windows(
        kv_padded[:, : local_groups * HEAD_DIM].reshape(padded_rows, local_groups, HEAD_DIM),
        rows_local,
        blocks,
    )
    block_values = block_windows(
        kv_padded[:, local_groups * HEAD_DIM :].reshape(padded_rows, local_groups, HEAD_DIM),
        rows_local,
        blocks,
    )
    scores = jnp.einsum(
        "nqkgd,nskd->nkgqs", block_queries, block_keys, preferred_element_type=jnp.float32
    ) * HEAD_DIM ** (-0.5)
    query_pos = positions.reshape(blocks, WINDOW)
    key_pos = (
        offset
        - WINDOW
        + (jnp.arange(blocks, dtype=jnp.int32) * WINDOW)[:, None]
        + jnp.arange(3 * WINDOW, dtype=jnp.int32)[None, :]
    )
    distance = key_pos[:, None, :] - query_pos[:, :, None]
    allowed = (
        (jnp.abs(distance) <= WINDOW)
        & (key_pos >= 0)[:, None, :]
        & (key_pos < total_tokens)[:, None, :]
    )
    scores = jnp.where(allowed[:, None, None], scores, -jnp.inf)
    sink_values = sink_logit.reshape(local_groups, group_size)[None, :, :, None]
    row_max = jnp.maximum(jnp.max(scores, axis=-1), sink_values)
    exp_scores = jnp.exp(scores - row_max[..., None])
    denominator = jnp.sum(exp_scores, axis=-1) + jnp.exp(sink_values - row_max)
    weights = (exp_scores / denominator[..., None]).astype(jnp.bfloat16)
    attended = (
        jnp.einsum("nkgqs,nskd->nqkgd", weights, block_values, preferred_element_type=jnp.float32)
        .astype(jnp.bfloat16)
        .reshape(rows_local, local_heads * HEAD_DIM)
    )
    log_sum = row_max + jnp.log(denominator)
    log_weight_sum = jnp.transpose(log_sum, (1, 2, 0, 3)).reshape(local_heads, rows_local)
    out_attn, out_conv = (
        lax.all_gather(w_out_attn, "sp", axis=1, tiled=True),
        lax.all_gather(w_out_conv, "sp", axis=1, tiled=True),
    )
    mixed = lax.psum_scatter(
        (
            jnp.dot(attended, out_attn, preferred_element_type=jnp.float32)
            + jnp.dot(conv_out, out_conv, preferred_element_type=jnp.float32)
        ).astype(jnp.bfloat16),
        "tp",
        scatter_dimension=0,
        tiled=True,
    )
    return (mixed, log_weight_sum)


def solution(mesh):
    placed = (
        P("sp", "tp"),
        P(),
        P("sp", "tp"),
        P("sp", "tp"),
        P("sp", "tp"),
        P("sp", "tp"),
        P("sp", "tp"),
        P("sp", "tp"),
        P(None, "tp"),
        P("tp"),
        P("tp", "sp"),
        P("tp", "sp"),
    )
    return jax.shard_map(
        on_device,
        mesh=mesh,
        in_specs=placed,
        out_specs=(P(("sp", "tp"), None), P("tp", "sp")),
        check_vma=False,
    )
```

profile of v0, /device:TPU:0, one launch (start us, length us, event | category | flops | bytes accessed | tf_op | source)
XLA Modules:
  0.0 326.0 jit_solution(14277394991578576114)
XLA Ops:
  13.0 34.2 %all_gather.29 = bf16[2048,64]{1,0:T(8,128)(2,1)S(1)} all-gather(bf16[256,64]{1,0:T(8,128)(2,1)S(1)} %copy.27), channel_id=1, replica_groups=mesh['sp'=8,'tp'=4] {'sp'}, dimensions={0}, use_global_device_ids=true | all-gather | bytes 294912 | tf_op jit(solution)/shard_map/all_gather | solution.py:90
  48.0 31.9 %all_gather.30 = bf16[2048,64]{1,0:T(8,128)(2,1)S(1)} all-gather(bf16[256,64]{1,0:T(8,128)(2,1)S(1)} %copy.28), channel_id=1, replica_groups=mesh['sp'=8,'tp'=4] {'sp'}, dimensions={0}, use_global_device_ids=true | all-gather | bytes 294912 | tf_op jit(solution)/shard_map/all_gather | solution.py:91
  79.9 1.4 fusion.91
  81.6 0.9 fusion.18
  82.6 14.6 %all-gather.12.cloned.1.call-done = bf16[2048,256]{1,0:T(8,128)(2,1)} async-done(((bf16[256,256]{1,0:T(8,128)(2,1)}), bf16[2048,256]{1,0:T(8,128)(2,1)}) %all-gather.12.cloned.1.call-update) | async-done | bytes 1048592 | tf_op jit(solution)/shard_map/all_gather | solution.py:92
  97.2 41.2 %all-gather.14.cloned.1.call-done = bf16[2048,256]{1,0:T(8,128)(2,1)} async-done(((bf16[256,256]{1,0:T(8,128)(2,1)}), bf16[2048,256]{1,0:T(8,128)(2,1)}) %all-gather.14.cloned.1.call-update) | async-done | bytes 1048592 | tf_op jit(solution)/shard_map/all_gather | solution.py:93
  138.4 41.0 %all-gather.16.cloned.1.call-done = bf16[2048,256]{1,0:T(8,128)(2,1)} async-done(((bf16[256,256]{1,0:T(8,128)(2,1)}), bf16[2048,256]{1,0:T(8,128)(2,1)}) %all-gather.16.cloned.1.call-update) | async-done | bytes 1048592 | tf_op jit(solution)/shard_map/all_gather | solution.py:94
  179.4 8.2 %concatenate.68 = bf16[2048,1152]{1,0:T(8,128)(2,1)} concatenate(bf16[2048,256]{1,0:T(8,128)(2,1)} %all-gather.10.cloned.1.call-done, bf16[2048,64]{1,0:T(8,128)(2,1)S(1)} %all_gather.29, bf16[2048,64]{1,0:T(8,128)(2,1)S(1)} %all_gather.30, bf16[2048,256]{1,0:T(8,128)(2,1)} %all-gather.12.cloned.1.call-done, bf16[2048,256]{1,0:T(8,128)(2,1)} %all-gather.14.cloned.1.call-done, ...), dimensions={1} | concatenate | bytes 9437184 | tf_op jit(solution)/shard_map/concatenate | solution.py:87
  187.6 14.5 %all-gather.8.cloned.1.call-done = bf16[512,2048]{1,0:T(8,128)(2,1)} async-done(((bf16[512,512]{1,0:T(8,128)(2,1)}), bf16[512,2048]{1,0:T(8,128)(2,1)}) %all-gather.8.cloned.1.call-update) | async-done | bytes 2097168 | tf_op jit(solution)/shard_map/all_gather | solution.py:74
  202.1 2.1 fusion
  204.2 5.9 %fusion.5 = f32[512,1152]{1,0:T(8,128)S(1)} fusion(bf16[2048,1152]{1,0:T(8,128)(2,1)} %concatenate.68, bf16[512,2048]{1,0:T(8,128)(2,1)} %all-gather.8.cloned.1.call-done, f32[2048]{0:T(1024)S(1)} %copy-done.7, f32[512]{0:T(512)S(1)} %add_rsqrt_fusion), kind=kOutput, calls=%fused_computation.11 | convolution fusion | flops 2420113408 | bytes 9185280 | tf_op jit(solution)/shard_map/dot_general | solution.py:98
  210.2 1.3 copy-done
  214.5 2.4 fusion.35
  217.1 3.4 %collective-permute-start = (bf16[128,128]{1,0:T(8,128)(2,1)S(1)}, bf16[128,128]{1,0:T(8,128)(2,1)S(1)}, u32[]{:S(2)}, u32[]{:S(2)}) collective-permute-start(bf16[128,128]{1,0:T(8,128)(2,1)S(1)} %get-tuple-element.24), channel_id=1, source_target_pairs={{0,4},{4,8},{8,12},{12,16},{16,20},{20,24},{24,28},{1,5},{5,9},{9,... | collective-permute-start | bytes 98312 | tf_op jit(solution)/shard_map/ppermute | solution.py:18
  220.5 1.3 collective-permute-start.1
  221.8 1.3 collective-permute-start.3
  223.1 5.2 %collective-permute-start.2 = (bf16[1,256]{1,0:T(2,128)(2,1)S(1)}, bf16[1,256]{1,0:T(2,128)(2,1)S(1)}, u32[]{:S(2)}, u32[]{:S(2)}) collective-permute-start(bf16[1,256]{1,0:T(2,128)(2,1)S(1)} %get-tuple-element.16), channel_id=1, source_target_pairs={{0,4},{4,8},{8,12},{12,16},{16,20},{20,24},{24,28},{1,5},{5,9},{9,... | collective-permute-start | bytes 1544 | tf_op jit(solution)/shard_map/ppermute | solution.py:18
  234.3 1.7 fusion.4
  236.0 1.6 copy.31
  240.4 3.1 all-gather.18.cloned.1.call-done
  243.4 4.1 %fusion.41 = f32[512,2048]{1,0:T(8,128)} fusion(bf16[256,2048]{1,0:T(8,128)(2,1)} %all-gather.18.cloned.1.call-done, bf16[32,8,4,128]{3,2,1,0:T(4,128)(2,1)S(1)} %bitcast.108), kind=kOutput, calls=%fused_computation.51 | convolution fusion | flops 536870912 | bytes 5505024 | tf_op jit(solution)/shard_map/dot_general | solution.py:181
  247.5 36.5 %all-gather.20.cloned.1.call-done = bf16[256,2048]{1,0:T(8,128)(2,1)} async-done(((bf16[256,256]{1,0:T(8,128)(2,1)}), bf16[256,2048]{1,0:T(8,128)(2,1)}) %all-gather.20.cloned.1.call-update) | async-done | bytes 1048592 | tf_op jit(solution)/shard_map/all_gather | solution.py:177
  284.0 4.8 %add_convert_fusion = bf16[512,2048]{1,0:T(8,128)(2,1)} fusion(f32[512,2048]{1,0:T(8,128)} %fusion.41, bf16[256,2048]{1,0:T(8,128)(2,1)} %all-gather.20.cloned.1.call-done, f32[514,256]{1,0:T(8,128)S(1)} %copy-done.1, f32[512,1152]{1,0:T(8,128)} %copy-done, f32[256]{0:T(256)S(1)} %bitcast.127, f32[256]{0:T(256)S(1)} %bitcast.128, f32[256]{0:T(256)S(1)} %bitcast.126), kind=kOutput, calls=%fused_computation.5 | convolution fusion | flops 539885568 | bytes 9440256 | tf_op jit(solution)/shard_map/dot_general | solution.py:182
  289.5 29.6 %reduce-scatter.2.cloned.1.call-done = bf16[128,2048]{1,0:T(8,128)(2,1)} async-done(((bf16[512,2048]{1,0:T(8,128)(2,1)}), bf16[128,2048]{1,0:T(8,128)(2,1)}) %reduce-scatter.2.cloned.1.call-update) | async-done | bytes 524304 | tf_op jit(solution)/shard_map/reduce_scatter | solution.py:179
  (74 shorter events, 19.6 us)
Async XLA Ops:
  7.2 75.5 %all-gather.10.cloned.1.call-start = ((), (), s32[]{:S(2)}) async-start(), calls=%async_computation.2 | async-start | bytes 1179648 | tf_op jit(solution)/shard_map/all_gather | solution.py:89
  7.9 89.3 %all-gather.12.cloned.1.call-start = ((), (), s32[]{:S(2)}) async-start(), calls=%async_computation.3 | async-start | bytes 1179648 | tf_op jit(solution)/shard_map/all_gather | solution.py:92
  8.6 129.7 %all-gather.14.cloned.1.call-start = ((), (), s32[]{:S(2)}) async-start(), calls=%async_computation.4 | async-start | bytes 1179648 | tf_op jit(solution)/shard_map/all_gather | solution.py:93
  9.4 170.0 %all-gather.16.cloned.1.call-start = ((), (), s32[]{:S(2)}) async-start(), calls=%async_computation.5 | async-start | bytes 1179648 | tf_op jit(solution)/shard_map/all_gather | solution.py:94
  10.0 192.2 %all-gather.8.cloned.1.call-start = ((), (), s32[]{:S(2)}) async-start(), calls=%async_computation.1 | async-start | bytes 2621440 | tf_op jit(solution)/shard_map/all_gather | solution.py:74
  10.5 232.9 %all-gather.18.cloned.1.call-start = ((), (), s32[]{:S(2)}) async-start(), calls=%async_computation.6 | async-start | bytes 1179648 | tf_op jit(solution)/shard_map/all_gather | solution.py:176
  11.1 272.9 %all-gather.20.cloned.1.call-start = ((), (), s32[]{:S(2)}) async-start(), calls=%async_computation.7 | async-start | bytes 1179648 | tf_op jit(solution)/shard_map/all_gather | solution.py:177
  11.9 307.3 %reduce-scatter.2.cloned.1.call-start = ((), (), s32[]{:S(2)}) async-start(), calls=%async_computation.8 | async-start | bytes 2621440 | tf_op jit(solution)/shard_map/reduce_scatter | solution.py:179
  82.6 121.6 %copy-start.7 = (f32[2048]{0:T(1024)S(1)}, f32[2048]{0:T(1024)}, u32[]{:S(2)}) copy-start(f32[2048]{0:T(1024)} %param.13) | copy-start | bytes 24580
  210.1 1.4 copy-start
  217.1 14.9 %collective-permute-start = (bf16[128,128]{1,0:T(8,128)(2,1)S(1)}, bf16[128,128]{1,0:T(8,128)(2,1)S(1)}, u32[]{:S(2)}, u32[]{:S(2)}) collective-permute-start(bf16[128,128]{1,0:T(8,128)(2,1)S(1)} %get-tuple-element.24), channel_id=1, source_target_pairs={{0,4},{4,8},{8,12},{12,16},{16,20},{20,24},{24,28},{1,5},{5,9},{9,... | collective-permute-start | bytes 98312 | tf_op jit(solution)/shard_map/ppermute | solution.py:18
  220.5 11.5 %collective-permute-start.1 = (bf16[128,128]{1,0:T(8,128)(2,1)S(1)}, bf16[128,128]{1,0:T(8,128)(2,1)S(1)}, u32[]{:S(2)}, u32[]{:S(2)}) collective-permute-start(bf16[128,128]{1,0:T(8,128)(2,1)S(1)} %get-tuple-element.25), channel_id=1, source_target_pairs={{4,0},{8,4},{12,8},{16,12},{20,16},{24,20},{28,24},{5,1},{9,5},{13... | collective-permute-start | bytes 98312 | tf_op jit(solution)/shard_map/ppermute | solution.py:21
  221.8 9.3 %collective-permute-start.3 = (bf16[1,256]{1,0:T(2,128)(2,1)S(1)}, bf16[1,256]{1,0:T(2,128)(2,1)S(1)}, u32[]{:S(2)}, u32[]{:S(2)}) collective-permute-start(bf16[1,256]{1,0:T(2,128)(2,1)S(1)} %get-tuple-element.17), channel_id=1, source_target_pairs={{4,0},{8,4},{12,8},{16,12},{20,16},{24,20},{28,24},{5,1},{9,5},{13... | collective-permute-start | bytes 1544 | tf_op jit(solution)/shard_map/ppermute | solution.py:21
  223.1 8.0 %collective-permute-start.2 = (bf16[1,256]{1,0:T(2,128)(2,1)S(1)}, bf16[1,256]{1,0:T(2,128)(2,1)S(1)}, u32[]{:S(2)}, u32[]{:S(2)}) collective-permute-start(bf16[1,256]{1,0:T(2,128)(2,1)S(1)} %get-tuple-element.16), channel_id=1, source_target_pairs={{0,4},{4,8},{8,12},{12,16},{16,20},{20,24},{24,28},{1,5},{5,9},{9,... | collective-permute-start | bytes 1544 | tf_op jit(solution)/shard_map/ppermute | solution.py:18
  232.8 5.5 %copy-start.4 = (f32[4]{0:T(128)S(1)}, f32[4]{0:T(128)}, u32[]{:S(2)}) copy-start(f32[4]{0:T(128)} %param.21) | copy-start | bytes 52
  238.3 0.8 copy-start.2
  238.3 0.9 copy-start.3
  243.4 40.6 %copy-start.1 = (f32[514,256]{1,0:T(8,128)S(1)}, f32[514,256]{1,0:T(8,128)}, u32[]{:S(2)}) copy-start(f32[514,256]{1,0:T(8,128)} %maximum_convert_fusion) | copy-start | bytes 1579012
  243.4 40.6 %copy-start.5 = (f32[1,256]{1,0:T(1,128)S(1)}, f32[1,256]{1,0:T(1,128)}, u32[]{:S(2)}) copy-start(f32[1,256]{1,0:T(1,128)} %get-tuple-element.27) | copy-start | bytes 3076
  243.4 40.6 %copy-start.6 = (f32[1,256]{1,0:T(1,128)S(1)}, f32[1,256]{1,0:T(1,128)}, u32[]{:S(2)}) copy-start(f32[1,256]{1,0:T(1,128)} %get-tuple-element.28) | copy-start | bytes 3076
Sparse Core Ops, SparseCore 0:
  10.1 45.7 all-gather.9
  58.0 39.1 all-gather.11
  99.4 38.9 all-gather.13
  140.4 38.9 all-gather.15
  180.8 21.2 all-gather.7
  204.0 39.3 all-gather.17
  245.5 38.4 all-gather.19
  288.9 30.1 reduce-scatter.1
where the time goes:
time: 327 us; the launch traced here: 326 us
  waiting for transfers between devices  185 us (57%)
  blocking collectives  66.1 us (20%)
  local copies, waits for them, and re-layouts  22.7 us (7%)
  matrix products  17.4 us (5%)
  between operations  14.4 us (4%)
  starting transfers between devices  11.4 us (3%)
  other arithmetic  9.22 us (3%)
    all_gather x1, waiting for transfers between devices, on_device(): lax.all_gather(w_pre_gate, 'sp', axis=0, tiled=True)  41.2 us
    all_gather x1, waiting for transfers between devices, on_device(): lax.all_gather(w_conv_in, 'sp', axis=0, tiled=True)  41 us
    all_gather x1, waiting for transfers between devices, on_device(): lax.all_gather(w_out_conv, 'sp', axis=1, tiled=True)  36.5 us
    all_gather x1, blocking collectives, on_device(): lax.all_gather(w_key, 'sp', axis=0, tiled=True)  34.2 us
    all_gather x1, blocking collectives, on_device(): lax.all_gather(w_value, 'sp', axis=0, tiled=True)  31.9 us
    reduce_scatter x1, waiting for transfers between devices, on_device(): lax.psum_scatter((jnp.dot(attended, out_attn, preferred_element_type=jnp....  29.6 us
    all_gather x1, waiting for transfers between devices, on_device(): lax.all_gather(w_post_gate, 'sp', axis=0, tiled=True)  14.6 us
    all_gather x1, waiting for transfers between devices, on_device(): whole = lax.all_gather(tokens, 'tp', axis=1, tiled=True)  14.5 us
  transfers between devices with their start and end apart: 12, of which 7 were waited for; matrix products, arithmetic and copies ran while one was open for 13% of the time, Pallas kernels for 0%

commit v1 on v0

--- a/solution.py
+++ b/solution.py
@@ -172,9 +172,12 @@
     )
     log_sum = row_max + jnp.log(denominator)
     log_weight_sum = jnp.transpose(log_sum, (1, 2, 0, 3)).reshape(local_heads, rows_local)
+    _rest_kinds = lambda field, which_dim: jnp.concatenate(
+        lax.all_gather(field, axis_name="sp"), axis=which_dim
+    )
     out_attn, out_conv = (
         lax.all_gather(w_out_attn, "sp", axis=1, tiled=True),
-        lax.all_gather(w_out_conv, "sp", axis=1, tiled=True),
+        _rest_kinds(w_out_conv, 1),
     )
     mixed = lax.psum_scatter(
         (

time: 327 us -> 328 us (level)
  waiting for transfers between devices: 185 us -> 199 us
  local copies, waits for them, and re-layouts: 22.7 us -> 15.4 us
  matrix products: 17.4 us -> 12.6 us
    all_gather x1, waiting for transfers between devices: 36.5 us -> 0.02 us  [on_device(): lax.all_gather(field, axis_name='sp')]
    all_gather x1, waiting for transfers between devices: 14.6 us -> 41.1 us  [on_device(): lax.all_gather(w_post_gate, 'sp', axis=0, tiled=True)]
    all_gather x1, waiting for transfers between devices: 0.02 us -> 13.8 us  [on_device(): lax.all_gather(w_query, 'sp', axis=0, tiled=True)]
    all_gather x1, waiting for transfers between devices: 3.06 us -> 13.1 us  [on_device(): lax.all_gather(w_out_attn, 'sp', axis=1, tiled=True)]
    concatenate x8, local copies, waits for them, and re-layouts: 5.27 us -> 0.41 us  [axial_rotate(): jnp.concatenate([rotate_pair(row_part, row_angle), rotate_pair(col_part,...]
    reshape x5, local copies, waits for them, and re-layouts: 3.89 us -> 0.56 us  [block_windows(): source[step * WINDOW:step * WINDOW + rows_local]]
  transfers between devices with their start and end apart: 12 -> 12, of which waited for: 7 -> 8; matrix products, arithmetic and copies ran while one was open for 13% -> 9% of each run, Pallas kernels for 0% -> 0%
where the time goes in v1:
time: 328 us; the launch traced here: 327 us
  waiting for transfers between devices  199 us (61%)
  blocking collectives  66.1 us (20%)
  local copies, waits for them, and re-layouts  15.4 us (5%)
  between operations  14.4 us (4%)
  matrix products  12.6 us (4%)
  starting transfers between devices  11.4 us (3%)
  other arithmetic  7.79 us (2%)
    all_gather x1, waiting for transfers between devices, on_device(): lax.all_gather(w_post_gate, 'sp', axis=0, tiled=True)  41.1 us
    all_gather x1, waiting for transfers between devices, on_device(): lax.all_gather(w_pre_gate, 'sp', axis=0, tiled=True)  41 us
    all_gather x1, waiting for transfers between devices, on_device(): lax.all_gather(w_conv_in, 'sp', axis=0, tiled=True)  41 us
    all_gather x1, blocking collectives, on_device(): lax.all_gather(w_key, 'sp', axis=0, tiled=True)  34.2 us
    all_gather x1, blocking collectives, on_device(): lax.all_gather(w_value, 'sp', axis=0, tiled=True)  31.9 us
    reduce_scatter x1, waiting for transfers between devices, on_device(): lax.psum_scatter((jnp.dot(attended, out_attn, preferred_element_type=jnp....  29.6 us
    all_gather x1, waiting for transfers between devices, on_device(): whole = lax.all_gather(tokens, 'tp', axis=1, tiled=True)  14.5 us
    all_gather x1, waiting for transfers between devices, on_device(): lax.all_gather(w_query, 'sp', axis=0, tiled=True)  13.8 us
  transfers between devices with their start and end apart: 12, of which 8 were waited for; matrix products, arithmetic and copies ran while one was open for 9% of the time, Pallas kernels for 0%

profile of v1, /device:TPU:0, one launch (start us, length us, event | category | flops | bytes accessed | tf_op | source)
XLA Modules:
  0.0 326.9 jit_solution(6766843247825071561)
XLA Ops:
  12.1 0.9 copy.46
  13.0 34.2 %all_gather.32 = bf16[2048,64]{1,0:T(8,128)(2,1)S(1)} all-gather(bf16[256,64]{1,0:T(8,128)(2,1)S(1)} %copy.46), channel_id=1, replica_groups=mesh['sp'=8,'tp'=4] {'sp'}, dimensions={0}, use_global_device_ids=true | all-gather | bytes 294912 | tf_op jit(solution)/shard_map/all_gather | solution.py:90
  48.0 31.9 %all_gather.33 = bf16[2048,64]{1,0:T(8,128)(2,1)S(1)} all-gather(bf16[256,64]{1,0:T(8,128)(2,1)S(1)} %copy.47), channel_id=1, replica_groups=mesh['sp'=8,'tp'=4] {'sp'}, dimensions={0}, use_global_device_ids=true | all-gather | bytes 294912 | tf_op jit(solution)/shard_map/all_gather | solution.py:91
  81.1 0.9 fusion.18
  82.0 1.5 copy.64
  83.5 13.8 %all-gather.11.cloned.1.call-done = bf16[2048,256]{1,0:T(8,128)(2,1)} async-done(((bf16[256,256]{1,0:T(8,128)(2,1)}), bf16[2048,256]{1,0:T(8,128)(2,1)}) %all-gather.11.cloned.1.call-update) | async-done | bytes 1048592 | tf_op jit(solution)/shard_map/all_gather | solution.py:89
  97.3 41.1 %all-gather.13.cloned.1.call-done = bf16[2048,256]{1,0:T(8,128)(2,1)} async-done(((bf16[256,256]{1,0:T(8,128)(2,1)}), bf16[2048,256]{1,0:T(8,128)(2,1)}) %all-gather.13.cloned.1.call-update) | async-done | bytes 1048592 | tf_op jit(solution)/shard_map/all_gather | solution.py:92
  138.4 41.0 %all-gather.15.cloned.1.call-done = bf16[2048,256]{1,0:T(8,128)(2,1)} async-done(((bf16[256,256]{1,0:T(8,128)(2,1)}), bf16[2048,256]{1,0:T(8,128)(2,1)}) %all-gather.15.cloned.1.call-update) | async-done | bytes 1048592 | tf_op jit(solution)/shard_map/all_gather | solution.py:93
  179.4 41.0 %all-gather.17.cloned.1.call-done = bf16[2048,256]{1,0:T(8,128)(2,1)} async-done(((bf16[256,256]{1,0:T(8,128)(2,1)}), bf16[2048,256]{1,0:T(8,128)(2,1)}) %all-gather.17.cloned.1.call-update) | async-done | bytes 1048592 | tf_op jit(solution)/shard_map/all_gather | solution.py:94
  220.4 8.2 %concatenate.68 = bf16[2048,1152]{1,0:T(8,128)(2,1)} concatenate(bf16[2048,256]{1,0:T(8,128)(2,1)} %all-gather.11.cloned.1.call-done, bf16[2048,64]{1,0:T(8,128)(2,1)S(1)} %all_gather.32, bf16[2048,64]{1,0:T(8,128)(2,1)S(1)} %all_gather.33, bf16[2048,256]{1,0:T(8,128)(2,1)} %all-gather.13.cloned.1.call-done, bf16[2048,256]{1,0:T(8,128)(2,1)} %all-gather.15.cloned.1.call-done, ...), dimensions={1} | concatenate | bytes 9437184 | tf_op jit(solution)/shard_map/concatenate | solution.py:87
  228.7 14.5 %all-gather.9.cloned.1.call-done = bf16[512,2048]{1,0:T(8,128)(2,1)} async-done(((bf16[512,512]{1,0:T(8,128)(2,1)}), bf16[512,2048]{1,0:T(8,128)(2,1)}) %all-gather.9.cloned.1.call-update) | async-done | bytes 2097168 | tf_op jit(solution)/shard_map/all_gather | solution.py:74
  243.2 2.1 fusion
  245.2 5.9 %fusion.5 = f32[512,1152]{1,0:T(8,128)S(1)} fusion(bf16[2048,1152]{1,0:T(8,128)(2,1)} %concatenate.68, bf16[512,2048]{1,0:T(8,128)(2,1)} %all-gather.9.cloned.1.call-done, f32[2048]{0:T(1024)S(1)} %copy-done.2, f32[512]{0:T(512)S(1)} %add_rsqrt_fusion), kind=kOutput, calls=%fused_computation.11 | convolution fusion | flops 2420113408 | bytes 9185280 | tf_op jit(solution)/shard_map/dot_general | solution.py:98
  251.3 1.3 copy-done
  253.1 2.4 fusion.35
  255.8 3.4 %collective-permute-start = (bf16[128,128]{1,0:T(8,128)(2,1)S(1)}, bf16[128,128]{1,0:T(8,128)(2,1)S(1)}, u32[]{:S(2)}, u32[]{:S(2)}) collective-permute-start(bf16[128,128]{1,0:T(8,128)(2,1)S(1)} %get-tuple-element.24), channel_id=1, source_target_pairs={{0,4},{4,8},{8,12},{12,16},{16,20},{20,24},{24,28},{1,5},{5,9},{9,... | collective-permute-start | bytes 98312 | tf_op jit(solution)/shard_map/ppermute | solution.py:18
  259.1 1.3 collective-permute-start.1
  260.4 1.3 collective-permute-start.3
  261.7 5.2 %collective-permute-start.2 = (bf16[1,256]{1,0:T(2,128)(2,1)S(1)}, bf16[1,256]{1,0:T(2,128)(2,1)S(1)}, u32[]{:S(2)}, u32[]{:S(2)}) collective-permute-start(bf16[1,256]{1,0:T(2,128)(2,1)S(1)} %get-tuple-element.16), channel_id=1, source_target_pairs={{0,4},{4,8},{8,12},{12,16},{16,20},{20,24},{24,28},{1,5},{5,9},{9,... | collective-permute-start | bytes 1544 | tf_op jit(solution)/shard_map/ppermute | solution.py:18
  270.4 1.0 fusion.14
  271.6 13.1 %all-gather.19.cloned.1.call-done = bf16[256,2048]{1,0:T(8,128)(2,1)} async-done(((bf16[256,256]{1,0:T(8,128)(2,1)}), bf16[256,2048]{1,0:T(8,128)(2,1)}) %all-gather.19.cloned.1.call-update) | async-done | bytes 1048592 | tf_op jit(solution)/shard_map/all_gather | solution.py:179
  284.7 2.0 fusion.41
  286.6 3.2 add_convert_fusion
  290.5 29.6 %reduce-scatter.2.cloned.1.call-done = bf16[128,2048]{1,0:T(8,128)(2,1)} async-done(((bf16[512,2048]{1,0:T(8,128)(2,1)}), bf16[128,2048]{1,0:T(8,128)(2,1)}) %reduce-scatter.2.cloned.1.call-update) | async-done | bytes 524304 | tf_op jit(solution)/shard_map/reduce_scatter | solution.py:182
  (65 shorter events, 12.0 us)
Async XLA Ops:
  7.2 74.9 %all-gather.21.cloned.1.call-start = ((), (), s32[]{:S(2)}) async-start(), calls=%async_computation.8 | async-start | bytes 1179648 | tf_op jit(solution)/shard_map/all_gather | solution.py:176
  7.9 89.4 %all-gather.11.cloned.1.call-start = ((), (), s32[]{:S(2)}) async-start(), calls=%async_computation.2 | async-start | bytes 1179648 | tf_op jit(solution)/shard_map/all_gather | solution.py:89
  8.6 129.8 %all-gather.13.cloned.1.call-start = ((), (), s32[]{:S(2)}) async-start(), calls=%async_computation.3 | async-start | bytes 1179648 | tf_op jit(solution)/shard_map/all_gather | solution.py:92
  9.4 170.0 %all-gather.15.cloned.1.call-start = ((), (), s32[]{:S(2)}) async-start(), calls=%async_computation.4 | async-start | bytes 1179648 | tf_op jit(solution)/shard_map/all_gather | solution.py:93
  10.0 210.5 %all-gather.17.cloned.1.call-start = ((), (), s32[]{:S(2)}) async-start(), calls=%async_computation.5 | async-start | bytes 1179648 | tf_op jit(solution)/shard_map/all_gather | solution.py:94
  10.5 232.6 %all-gather.9.cloned.1.call-start = ((), (), s32[]{:S(2)}) async-start(), calls=%async_computation.1 | async-start | bytes 2621440 | tf_op jit(solution)/shard_map/all_gather | solution.py:74
  11.1 273.5 %all-gather.19.cloned.1.call-start = ((), (), s32[]{:S(2)}) async-start(), calls=%async_computation.6 | async-start | bytes 1179648 | tf_op jit(solution)/shard_map/all_gather | solution.py:179
  11.9 308.2 %reduce-scatter.2.cloned.1.call-start = ((), (), s32[]{:S(2)}) async-start(), calls=%async_computation.7 | async-start | bytes 2621440 | tf_op jit(solution)/shard_map/reduce_scatter | solution.py:182
  83.5 161.7 %copy-start.2 = (f32[2048]{0:T(1024)S(1)}, f32[2048]{0:T(1024)}, u32[]{:S(2)}) copy-start(f32[2048]{0:T(1024)} %param.13) | copy-start | bytes 24580
  251.2 1.4 copy-start
  255.8 12.5 %collective-permute-start = (bf16[128,128]{1,0:T(8,128)(2,1)S(1)}, bf16[128,128]{1,0:T(8,128)(2,1)S(1)}, u32[]{:S(2)}, u32[]{:S(2)}) collective-permute-start(bf16[128,128]{1,0:T(8,128)(2,1)S(1)} %get-tuple-element.24), channel_id=1, source_target_pairs={{0,4},{4,8},{8,12},{12,16},{16,20},{20,24},{24,28},{1,5},{5,9},{9,... | collective-permute-start | bytes 98312 | tf_op jit(solution)/shard_map/ppermute | solution.py:18
  259.1 9.2 %collective-permute-start.1 = (bf16[128,128]{1,0:T(8,128)(2,1)S(1)}, bf16[128,128]{1,0:T(8,128)(2,1)S(1)}, u32[]{:S(2)}, u32[]{:S(2)}) collective-permute-start(bf16[128,128]{1,0:T(8,128)(2,1)S(1)} %get-tuple-element.25), channel_id=1, source_target_pairs={{4,0},{8,4},{12,8},{16,12},{20,16},{24,20},{28,24},{5,1},{9,5},{13... | collective-permute-start | bytes 98312 | tf_op jit(solution)/shard_map/ppermute | solution.py:21
  260.4 7.0 %collective-permute-start.3 = (bf16[1,256]{1,0:T(2,128)(2,1)S(1)}, bf16[1,256]{1,0:T(2,128)(2,1)S(1)}, u32[]{:S(2)}, u32[]{:S(2)}) collective-permute-start(bf16[1,256]{1,0:T(2,128)(2,1)S(1)} %get-tuple-element.17), channel_id=1, source_target_pairs={{4,0},{8,4},{12,8},{16,12},{20,16},{24,20},{28,24},{5,1},{9,5},{13... | collective-permute-start | bytes 1544 | tf_op jit(solution)/shard_map/ppermute | solution.py:21
  261.7 6.5 %collective-permute-start.2 = (bf16[1,256]{1,0:T(2,128)(2,1)S(1)}, bf16[1,256]{1,0:T(2,128)(2,1)S(1)}, u32[]{:S(2)}, u32[]{:S(2)}) collective-permute-start(bf16[1,256]{1,0:T(2,128)(2,1)S(1)} %get-tuple-element.16), channel_id=1, source_target_pairs={{0,4},{4,8},{8,12},{12,16},{16,20},{20,24},{24,28},{1,5},{5,9},{9,... | collective-permute-start | bytes 1544 | tf_op jit(solution)/shard_map/ppermute | solution.py:18
  268.4 1.1 copy-start.1
Sparse Core Ops, SparseCore 0:
  10.1 45.7 all-gather.20
  58.0 39.2 all-gather.10
  99.5 38.9 all-gather.12
  140.4 38.9 all-gather.14
  181.4 38.9 all-gather.16
  221.8 21.2 all-gather.8
  245.2 39.4 all-gather.18
  289.9 30.0 reduce-scatter.1
